TPU v7x, 32 devices: a whole 2x2x4 slice. The times are simulated.
32 devices in a mesh: sp: 8 (over z, y), tp: 4 (over x, core).
Axes of the slice: x: 2, y: 2, z: 4, core: 2. Of those that a mesh axis runs over, the one named last changes fastest.
Arguments:
- residual: bfloat16 [4, 768, 2048], P('tp', 'sp'), may hold values from -3 to 3
- query_nope: bfloat16 [4, 768, 1024], P('tp', 'sp'), may hold values from -9 to 9
- query_rope: bfloat16 [4, 768, 512], P('tp', 'sp'), may hold values from -48 to 48
- latent: bfloat16 [4, 768, 128], P('tp', 'sp'), may hold values from -6 to 6
- rope_key: bfloat16 [4, 768, 32], P('tp', 'sp'), may hold values from -48 to 48
- latent_gain: float32 [128], replicated, may hold values from 0.1 to 1.9
- up_key: bfloat16 [128, 1024], replicated, may hold values from -1 to 1
- up_value: bfloat16 [128, 1024], replicated, may hold values from -0.5 to 0.5
- out_weight: bfloat16 [1024, 2048], replicated, may hold values from -0.375 to 0.375
- ffn_gain: float32 [2048], replicated, may hold values from 0.1 to 1.9
- routes: int32 [4, 768, 2], P(None, 'sp'), may hold values from 0 to 7, all different within a row; in each aligned block of 96 rows (0 to 95, 96 to 191, ..., all dimensions but the last counted through in order) at most 30 rows name the same one
- route_weight: float32 [4, 768, 2], P('tp', 'sp'), may hold values from 0.1 to 1
- gate_weight: bfloat16 [8, 2048, 1024], P('sp', None, 'tp'), may hold values from -1.5 to 1.5
- up_weight: bfloat16 [8, 2048, 1024], P('sp', None, 'tp'), may hold values from -1.5 to 1.5
- down_weight: bfloat16 [8, 1024, 2048], P('sp', 'tp'), may hold values from -0.046875 to 0.046875
Outputs:
- updated: bfloat16 [4, 768, 2048], P('tp', 'sp')
Inputs may be any that keep to these rules, and one draw needn't show every extreme that they name: `routes`: each row names 2 different experts. In each aligned block of 96 rows (one sequence's rows of one device) no expert is named by more than 30 rows, a bound that some block reaches.
All inputs are finite; a program needn't handle non-finite values.
Results may differ from a plain program's by a relative error of at most 0.017.
Values may be sent and summed in bfloat16 or wider, within the bound.
A program may use at most 64 MiB of HBM per device.

v0:
```python
import functools

import jax
import jax.numpy as jnp
from jax import lax
from jax.experimental import pallas as pl
from jax.experimental.pallas import tpu as pltpu
from jax.sharding import PartitionSpec as P

HEADS = 16
NOPE = 64
ROPE = 32
VDIM = 64
LATENT = 128
TOPK = 2
LANES = 128

EPS = 1e-06
ROPE_BASE = 10000.0
CLAMP = 7.0
ALPHA = 1.702
MESH = pl.DeviceIdType.MESH
VM = pl.BlockSpec(memory_space=pltpu.VMEM)
F32 = jnp.float32
BF16 = jnp.bfloat16


def swapped(x):
    lane = lax.broadcasted_iota(jnp.int32, x.shape, 1)
    half = ROPE // 2
    return jnp.where(
        lane % ROPE < half, pltpu.roll(x, x.shape[1] - half, 1), pltpu.roll(x, half, 1)
    )


def prep_kernel(lat_ref, gain_ref, rk_ref, cos_ref, sin_ref, blk_ref):
    lat = lat_ref[...].astype(F32)
    mean = jnp.mean(lat * lat, axis=-1, keepdims=True)
    blk_ref[:, :LATENT] = (lat * lax.rsqrt(mean + EPS) * gain_ref[...]).astype(BF16)
    rk = rk_ref[...].astype(F32)
    blk_ref[:, LATENT:] = (rk * cos_ref[...] + swapped(rk) * sin_ref[...]).astype(BF16)


def place(picks_ref, experts, slots, tokens):
    expert = lax.broadcasted_iota(jnp.int32, (experts, tokens), 0)
    hots = [(expert == picks_ref[k : k + 1, :]).astype(F32) for k in range(TOPK)]
    earlier = (
        lax.broadcasted_iota(jnp.int32, (tokens, tokens), 0)
        < lax.broadcasted_iota(jnp.int32, (tokens, tokens), 1)
    ).astype(F32)
    rank = jnp.dot(sum(hots), earlier, preferred_element_type=F32)
    where = rank + (expert * slots).astype(F32)
    slot = lax.broadcasted_iota(jnp.int32, (experts * slots, tokens), 0).astype(F32)
    return [
        (slot == jnp.sum(hot * where, axis=0, keepdims=True)).astype(F32) for hot in hots
    ]


def attend_kernel(
    n, slots,
    blk_ref, qn_ref, qr_ref, cos_ref, sin_ref, upk_ref, upv_ref, ow_ref, res_ref, gain_ref,
    picks_ref, mid_ref, out_ref, rows, qrot, att, norm, send_sem, recv_sem,
):
    tokens = blk_ref.shape[0]
    width = res_ref.shape[1]
    me = lax.axis_index("sp")
    barrier = pltpu.get_barrier_semaphore()
    for d in range(1, n):
        pl.semaphore_signal(
            barrier, inc=1, device_id={"sp": lax.rem(me + d, n)}, device_id_type=MESH
        )
    pl.semaphore_wait(barrier, n - 1)
    copies = []
    for d in range(1, n):
        copy = pltpu.make_async_remote_copy(
            src_ref=blk_ref,
            dst_ref=rows.at[pl.ds(d * tokens, tokens)],
            send_sem=send_sem.at[d],
            recv_sem=recv_sem.at[d],
            device_id={"sp": lax.rem(me + d, n)},
            device_id_type=MESH,
        )
        copy.start()
        copies.append(copy)
    rows[:tokens, :] = blk_ref[...]
    for g in range(HEADS * ROPE // LANES):
        x = qr_ref[:, g * LANES : (g + 1) * LANES].astype(F32)
        qrot[:, g * LANES : (g + 1) * LANES] = (
            x * cos_ref[...] + swapped(x) * sin_ref[...]
        ).astype(BF16)
    factor = (NOPE + ROPE) ** (-0.5)
    lane = lax.broadcasted_iota(jnp.int32, (tokens, LANES), 1)
    low = lane < NOPE
    lowb = low.astype(F32).astype(BF16)
    highb = (lane >= NOPE).astype(F32).astype(BF16)
    ropeb = [(lane // ROPE == k).astype(F32).astype(BF16) for k in range(LANES // ROPE)]
    for copy in copies:
        copy.wait()

    def group(g, carry):
        turned = qrot[:, pl.ds(pl.multiple_of(g * LANES, LANES), LANES)]
        for q in range(2):
            lanes = pl.ds(pl.multiple_of((g * 2 + q) * LANES, LANES), LANES)
            lat = rows[:, :LATENT]
            keys = jnp.dot(lat, upk_ref[:, lanes], preferred_element_type=F32).astype(BF16)
            vals = jnp.dot(lat, upv_ref[:, lanes], preferred_element_type=F32).astype(BF16)
            keys = jnp.concatenate([keys, rows[:, LATENT:]], axis=1)
            plain = qn_ref[:, lanes]
            first = jnp.concatenate([plain * lowb, turned * ropeb[2 * q]], axis=1)
            second = jnp.concatenate([plain * highb, turned * ropeb[2 * q + 1]], axis=1)
            query = jnp.concatenate([first, second], axis=0)
            scores = lax.dot_general(
                query, keys, (((1,), (1,)), ((), ())), preferred_element_type=F32
            ) * factor
            weights = jnp.exp(scores - jnp.max(scores, axis=-1, keepdims=True))
            total = jnp.sum(weights, axis=-1, keepdims=True)
            mixed = jnp.dot(weights.astype(BF16), vals, preferred_element_type=F32) / total
            att[:, lanes] = jnp.where(low, mixed[:tokens], mixed[tokens:]).astype(BF16)
        return carry

    lax.fori_loop(0, HEADS * ROPE // LANES, group, 0)
    step = 512

    def project(c, square):
        cols = pl.ds(pl.multiple_of(c * step, step), step)
        product = jnp.dot(att[...], ow_ref[:, cols], preferred_element_type=F32)
        middle = (res_ref[:, cols].astype(F32) + product).astype(BF16)
        mid_ref[:, cols] = middle
        wide = middle.astype(F32)
        return square + jnp.sum(wide * wide, axis=-1, keepdims=True)

    square = lax.fori_loop(0, width // step, project, jnp.zeros((tokens, 1), F32))
    scale = lax.rsqrt(square / width + EPS)
    norm[...] = (mid_ref[...].astype(F32) * scale * gain_ref[...]).astype(BF16)
    packer = sum(place(picks_ref, n, slots, tokens)).astype(BF16)

    def pack(c, carry):
        cols = pl.ds(pl.multiple_of(c * step, step), step)
        out_ref[:, cols] = jnp.dot(packer, norm[:, cols], preferred_element_type=F32).astype(BF16)
        return carry

    lax.fori_loop(0, width // step, pack, 0)


def expert_kernel(
    n, m, slots,
    sent_ref, gate_ref, up_ref, down_ref, mid_ref, picks_ref, weight_ref, out_ref,
    held, red, fin, back, local_sem, send_sem, recv_sem,
):
    tokens, width = mid_ref.shape
    groups = m // 2
    me = lax.axis_index("sp")
    rank = lax.axis_index("tp")
    sibling = rank + 1 - 2 * lax.rem(rank, 2)
    parts = min(4, n)
    count = n // parts
    span = count * slots
    step = 512
    barrier = pltpu.get_barrier_semaphore()
    for d in range(1, n):
        pl.semaphore_signal(
            barrier, inc=1, device_id={"sp": lax.rem(me + d, n)}, device_id_type=MESH
        )
    for j in range(1, groups):
        pl.semaphore_signal(
            barrier, inc=1, device_id={"tp": lax.rem(rank + 2 * j, m)}, device_id_type=MESH
        )
    pl.semaphore_signal(barrier, inc=1, device_id={"tp": sibling}, device_id_type=MESH)
    pl.semaphore_wait(barrier, n + groups - 1)
    used = [0]

    def remote(source, target, device):
        index = used[0]
        used[0] += 1
        copy = pltpu.make_async_remote_copy(
            src_ref=source,
            dst_ref=target,
            send_sem=send_sem.at[index],
            recv_sem=recv_sem.at[index],
            device_id=device,
            device_id_type=MESH,
        )
        copy.start()
        return copy

    first = pltpu.make_async_copy(
        sent_ref.at[pl.ds(me * slots, slots)], held.at[0, 0, pl.ds(0, slots)], local_sem
    )
    first.start()
    arrive = [first]
    for d in range(1, n):
        peer = lax.rem(me + d, n)
        arrive.append(
            remote(
                sent_ref.at[pl.ds(peer * slots, slots)],
                held.at[0, 0, pl.ds(d * slots, slots)],
                {"sp": peer},
            )
        )
    across, aside, reduced, final, returned = {}, {}, {}, {}, {}

    def forward(k):
        rows = pl.ds(k * span, span)
        for d in range(k * count, (k + 1) * count):
            arrive[d].wait()
        for j in range(1, groups):
            across[k, j] = remote(
                held.at[0, 0, rows], held.at[j, 0, rows], {"tp": lax.rem(rank + 2 * j, m)}
            )
        aside[k, 0] = remote(held.at[0, 0, rows], held.at[0, 1, rows], {"tp": sibling})

    def relay(k):
        rows = pl.ds(k * span, span)
        for j in range(1, groups):
            across[k, j].wait()
            aside[k, j] = remote(held.at[j, 0, rows], held.at[j, 1, rows], {"tp": sibling})

    def compute(k):
        rows = pl.ds(k * span, span)
        for j in range(groups):
            aside[k, j].wait()
        block = jnp.concatenate(
            [held[j, c, rows, :] for j in range(groups) for c in range(2)], axis=0
        )
        gate = jnp.minimum(jnp.dot(block, gate_ref[...], preferred_element_type=F32), CLAMP)
        lift = jnp.clip(
            jnp.dot(block, up_ref[...], preferred_element_type=F32), -CLAMP, CLAMP
        )
        active = (gate * jax.nn.sigmoid(ALPHA * gate) * (lift + 1.0)).astype(BF16)

        def down(c, carry):
            cols = pl.ds(pl.multiple_of(c * step, step), step)
            term = jnp.dot(active, down_ref[:, cols], preferred_element_type=F32).astype(BF16)
            for i in range(m):
                held[i // 2, i % 2, rows, cols] = term[i * span : (i + 1) * span]
            return carry

        lax.fori_loop(0, width // step, down, 0)
        for j in range(groups):
            reduced[k, j] = remote(held.at[j, 1, rows], red.at[j, rows], {"tp": sibling})

    def reduce(k):
        rows = pl.ds(k * span, span)
        for j in list(range(1, groups)) + [0]:
            reduced[k, j].wait()
            total = held[j, 0, rows, :].astype(F32) + red[j, rows, :].astype(F32)
            held[j, 0, rows, :] = total.astype(BF16)
            if j:
                final[k, j] = remote(
                    held.at[j, 0, rows], fin.at[j - 1, rows], {"tp": lax.rem(rank + m - 2 * j, m)}
                )

    def finish(k):
        rows = pl.ds(k * span, span)
        total = held[0, 0, rows, :].astype(F32)
        for j in range(1, groups):
            final[k, j].wait()
            total = total + fin[j - 1, rows, :].astype(F32)
        held[0, 0, rows, :] = total.astype(BF16)
        for d in range(k * count, (k + 1) * count):
            source = held.at[0, 0, pl.ds(d * slots, slots)]
            target = back.at[pl.ds(me * slots, slots)]
            if d:
                returned[d] = remote(source, target, {"sp": lax.rem(me + n - d, n)})
            else:
                returned[d] = pltpu.make_async_copy(source, target, local_sem)
                returned[d].start()

    for t in range(parts + 4):
        for work, k in ((forward, t), (relay, t - 1), (compute, t - 2), (reduce, t - 3), (finish, t - 4)):
            if 0 <= k < parts:
                work(k)
    spots = place(picks_ref, n, slots, tokens)
    high = low = 0.0
    for k in range(TOPK):
        weight = weight_ref[k : k + 1, :]
        coarse = weight.astype(BF16).astype(F32)
        high = high + spots[k] * coarse
        low = low + spots[k] * (weight - coarse)
    high = high.astype(BF16)
    low = low.astype(BF16)
    dims = (((0,), (0,)), ((), ()))
    for d in range(n):
        returned[d].wait()

    def chunk(c, carry):
        cols = pl.ds(pl.multiple_of(c * step, step), step)
        rows = back[:, cols]
        added = lax.dot_general(high, rows, dims, preferred_element_type=F32)
        added = added + lax.dot_general(low, rows, dims, preferred_element_type=F32)
        out_ref[:, cols] = (mid_ref[:, cols].astype(F32) + added).astype(BF16)
        return carry

    lax.fori_loop(0, width // step, chunk, 0)


def local(
    residual, query_nope, query_rope, latent, rope_key, latent_gain, up_key, up_value,
    out_weight, ffn_gain, routes, route_weight, gate_weight, up_weight, down_weight,
):
    tokens, width = residual.shape[1:]
    n = lax.axis_size("sp")
    slots = min(tokens, max(2, 5 * tokens * TOPK // (4 * n)))
    slots = -(-slots // 16) * 16
    positions = lax.axis_index("sp") * tokens + jnp.arange(tokens, dtype=jnp.int32)
    lane = jnp.arange(LANES, dtype=jnp.int32)
    half = ROPE // 2
    inverse = ROPE_BASE ** (-(lane % half).astype(F32) * 2.0 / ROPE)
    angle = positions.astype(F32)[:, None] * inverse[None, :]
    cosine = jnp.cos(angle)
    sine = jnp.sin(angle) * jnp.where(lane % ROPE < half, -1.0, 1.0)[None, :]
    blk = pl.pallas_call(
        prep_kernel,
        out_shape=jax.ShapeDtypeStruct((tokens, 2 * LANES), BF16),
        in_specs=[VM] * 5,
        out_specs=VM,
    )(latent[0], latent_gain[None, :], jnp.tile(rope_key[0], (1, LANES // ROPE)), cosine, sine)
    picks = lax.dynamic_index_in_dim(
        jnp.transpose(routes, (0, 2, 1)), lax.axis_index("tp"), 0, keepdims=False
    )
    middle, outgoing = pl.pallas_call(
        functools.partial(attend_kernel, n, slots),
        out_shape=(
            jax.ShapeDtypeStruct((tokens, width), BF16),
            jax.ShapeDtypeStruct((n * slots, width), BF16),
        ),
        in_specs=[VM] * 11,
        out_specs=(VM, VM),
        scratch_shapes=[
            pltpu.VMEM((n * tokens, 2 * LANES), BF16),
            pltpu.VMEM((tokens, HEADS * ROPE), BF16),
            pltpu.VMEM((tokens, HEADS * VDIM), BF16),
            pltpu.VMEM((tokens, width), BF16),
            pltpu.SemaphoreType.DMA((n,)),
            pltpu.SemaphoreType.DMA((n,)),
        ],
        compiler_params=pltpu.CompilerParams(
            collective_id=0, has_side_effects=True, vmem_limit_bytes=60 * 2**20
        ),
    )(
        blk, query_nope[0], query_rope[0], cosine, sine, up_key, up_value, out_weight,
        residual[0], ffn_gain[None, :], picks,
    )
    m = lax.axis_size("tp")
    copies = 2 * (n - 1) + min(4, n) * (4 * (m // 2) - 2)
    updated = pl.pallas_call(
        functools.partial(expert_kernel, n, m, slots),
        out_shape=jax.ShapeDtypeStruct((tokens, width), BF16),
        in_specs=[VM] * 7,
        out_specs=VM,
        scratch_shapes=[
            pltpu.VMEM((m // 2, 2, n * slots, width), BF16),
            pltpu.VMEM((m // 2, n * slots, width), BF16),
            pltpu.VMEM((max(1, m // 2 - 1), n * slots, width), BF16),
            pltpu.VMEM((n * slots, width), BF16),
            pltpu.SemaphoreType.DMA,
            pltpu.SemaphoreType.DMA((copies,)),
            pltpu.SemaphoreType.DMA((copies,)),
        ],
        compiler_params=pltpu.CompilerParams(
            collective_id=1, has_side_effects=True, vmem_limit_bytes=60 * 2**20
        ),
    )(
        outgoing, gate_weight[0], up_weight[0], down_weight[0], middle, picks,
        jnp.transpose(route_weight[0], (1, 0)),
    )
    return updated[None]


def solution(mesh):
    in_specs = (
        P("tp", "sp", None),
        P("tp", "sp", None),
        P("tp", "sp", None),
        P("tp", "sp", None),
        P("tp", "sp", None),
        P(),
        P(),
        P(),
        P(),
        P(),
        P(None, "sp", None),
        P("tp", "sp", None),
        P("sp", None, "tp"),
        P("sp", None, "tp"),
        P("sp", "tp", None),
    )
    out_specs = P("tp", "sp", None)
    return jax.shard_map(local, mesh=mesh, in_specs=in_specs, out_specs=out_specs, check_vma=False)
```

profile of v0, /device:TPU:0, one launch (start us, length us, event | category | flops | bytes accessed | tf_op | source)
XLA Modules:
  0.0 113.0 jit_solution(10924900531564826999)
XLA Ops:
  0.0 0.0 copy-start
  0.0 0.7 copy-done
  0.7 0.6 dynamic-slice_bitcast_fusion.picks_ref
  1.3 0.7 tile.11
  2.0 0.7 copy.17.rk_ref
  2.7 0.9 fusion
  3.6 1.6 %shard_map.145.blk_ref = bf16[96,256]{1,0:T(8,128)(2,1)} custom-call(bf16[96,128]{1,0:T(8,128)(2,1)} %bitcast.27, f32[1,128]{1,0:T(1,128)} %bitcast.31, bf16[96,128]{1,0:T(8,128)(2,1)} %copy.17.rk_ref, f32[96,128]{1,0:T(8,128)} %get-tuple-element.10.cos_ref, f32[96,128]{1,0:T(8,128)} %get-tuple-element.9.sin_ref), custom_call_target="tpu_custom_call" | custom-call | tf_op jit(solution)/shard_map/pallas_call | solution.py:312
  5.2 24.5 %shard_map.146 = (bf16[96,2048]{1,0:T(8,128)(2,1)}, bf16[256,2048]{1,0:T(8,128)(2,1)}) custom-call(bf16[96,256]{1,0:T(8,128)(2,1)} %shard_map.145.blk_ref, bf16[96,1024]{1,0:T(8,128)(2,1)} %bitcast.24, bf16[96,512]{1,0:T(8,128)(2,1)} %bitcast.26, f32[96,128]{1,0:T(8,128)} %get-tuple-element.10.cos_ref, f32[96,128]{1,0:T(8,128)} %get-tuple-element.9.sin_ref, ...), custom_call_target="tpu_custom_call" | custom-call | tf_op jit(solution)/shard_map/pallas_call | solution.py:321
  29.7 81.5 %shard_map.147 = bf16[96,2048]{1,0:T(8,128)(2,1)} custom-call(bf16[256,2048]{1,0:T(8,128)(2,1)} %get-tuple-element.7.sent_ref, bf16[2048,256]{1,0:T(8,128)(2,1)} %bitcast.20, bf16[2048,256]{1,0:T(8,128)(2,1)} %bitcast.21, bf16[256,2048]{1,0:T(8,128)(2,1)} %bitcast.22, bf16[96,2048]{1,0:T(8,128)(2,1)} %get-tuple-element.8.mid_ref, ...), custom_call_target="tpu_custom_call" | custom-call | tf_op jit(solution)/shard_map/pallas_call | solution.py:346
  111.2 1.8 %copy.19 = bf16[1,96,2048]{2,1,0:T(8,128)(2,1)} copy(bf16[1,96,2048]{2,1,0:T(8,128)(2,1)} %bitcast.19) | data formatting | bytes 786432
  (2 shorter events, 0.0 us)
Async XLA Ops:
  0.0 0.7 copy-start
where the time goes:
time: 113 us
  Pallas kernels  108 us (96%)
  local copies, waits for them, and re-layouts  4.44 us (4%)
    pallas_call x1, Pallas kernels, local(): pl.pallas_call(functools.partial(expert_kernel, n, m, slots), out_shape=j...  81.5 us
    pallas_call x1, Pallas kernels, local(): pl.pallas_call(functools.partial(attend_kernel, n, slots), out_shape=(jax...  24.5 us
    unnamed x3, local copies, waits for them, and re-layouts  2.45 us

commit v1 on v0

v1 whole, which is shorter than its diff:
```python
import functools

import jax
import jax.numpy as jnp
import numpy as np
from jax import lax
from jax.experimental import pallas as pl
from jax.experimental.pallas import tpu as pltpu
from jax.sharding import PartitionSpec as P

HEADS = 16
NOPE = 64
ROPE = 32
VDIM = 64
LATENT = 128
TOPK = 2
LANES = 128

EPS = 1e-06
ROPE_BASE = 10000.0
CLAMP = 7.0
ALPHA = 1.702
LOG2E = 1.4426950408889634
MESH = pl.DeviceIdType.MESH
VM = pl.BlockSpec(memory_space=pltpu.VMEM)
ANY = pl.BlockSpec(memory_space=pl.ANY)
F32 = jnp.float32
BF16 = jnp.bfloat16
BYCOL = (((1,), (1,)), ((), ()))


def swapped(x):
    lane = lax.broadcasted_iota(jnp.int32, x.shape, 1)
    half = ROPE // 2
    return jnp.where(
        lane % ROPE < half, pltpu.roll(x, x.shape[1] - half, 1), pltpu.roll(x, half, 1)
    )


def place(picks_ref, experts, slots, tokens):
    expert = lax.broadcasted_iota(jnp.int32, (experts, tokens), 0)
    hots = [(expert == picks_ref[k : k + 1, :]).astype(F32) for k in range(TOPK)]
    earlier = (
        lax.broadcasted_iota(jnp.int32, (tokens, tokens), 0)
        < lax.broadcasted_iota(jnp.int32, (tokens, tokens), 1)
    ).astype(F32)
    rank = jnp.dot(sum(hots), earlier, preferred_element_type=F32)
    where = rank + (expert * slots).astype(F32)
    slot = lax.broadcasted_iota(jnp.int32, (experts * slots, tokens), 0).astype(F32)
    return [
        (slot == jnp.sum(hot * where, axis=0, keepdims=True)).astype(F32) for hot in hots
    ]


def partners(me, d, n):
    if n & (n - 1):
        return lax.rem(me + d, n), lax.rem(me + n - d, n)
    peer, bit = me, 1
    while bit < n:
        if d & bit:
            peer = peer + bit * (1 - 2 * lax.rem(lax.div(me, bit), 2))
        bit *= 2
    return peer, peer


def layer_kernel(
    n, m, slots, parts,
    lat_any, rope_any, lgain_any, tab_any, qn_any, qr_any, upk_any, upv_any, ow_any, res_any,
    fgain_any, routes_any, share_any, gate_any, up_any, down_any,
    out_ref,
    lat_ref, rope_ref, lgain_ref, tab_ref, qn_ref, qr_ref, upk_ref, upv_ref, ow_ref, mid_ref,
    fgain_ref, picks_ref, share_ref, gu_ref, dw_ref,
    kv, keys, vals, query, att, norm, packer, high, low, sent, rows_a, rows_b, act, act_b, res, back,
    load_sem, send_sem, recv_sem,
):
    tokens, width = out_ref.shape
    hidden = gate_any.shape[1]
    groups = m // 2
    local = 2 * hidden
    me = lax.axis_index("sp")
    rank = lax.axis_index("tp")
    sibling = rank + 1 - 2 * lax.rem(rank, 2)
    count = n // parts
    span = count * slots
    step = 512
    order = list(range(n - 1, -1, -1))
    packed = tokens // (LANES // ROPE)

    barrier = pltpu.get_barrier_semaphore()
    for d in range(1, n):
        pl.semaphore_signal(
            barrier, inc=1, device_id={"sp": partners(me, d, n)[0]}, device_id_type=MESH
        )
    for j in range(1, groups):
        pl.semaphore_signal(
            barrier, inc=1, device_id={"tp": lax.rem(rank + 2 * j, m)}, device_id_type=MESH
        )
    pl.semaphore_signal(barrier, inc=1, device_id={"tp": sibling}, device_id_type=MESH)

    loads = {}

    def load(name, source, target):
        loads[name] = pltpu.make_async_copy(source, target, load_sem.at[len(loads)])
        loads[name].start()

    load("lat", lat_any, lat_ref)
    load("rope", rope_any, rope_ref)
    load("lgain", lgain_any, lgain_ref)
    load("tab", tab_any, tab_ref)
    load("qr", qr_any, qr_ref)
    load("qn", qn_any, qn_ref)
    load("upk", upk_any, upk_ref)
    load("picks", routes_any.at[rank], picks_ref)
    load("share", share_any, share_ref)
    load("upv", upv_any, upv_ref)
    load("ow", ow_any, ow_ref)
    load("res", res_any, mid_ref)
    load("fgain", fgain_any, fgain_ref)
    load("gate", gate_any, gu_ref.at[:, pl.ds(0, hidden)])
    load("up", up_any, gu_ref.at[:, pl.ds(local, hidden)])
    load("down", down_any, dw_ref.at[pl.ds(0, hidden)])

    used = [0]

    def remote(source, target, device):
        index = used[0]
        used[0] += 1
        copy = pltpu.make_async_remote_copy(
            src_ref=source,
            dst_ref=target,
            send_sem=send_sem.at[index],
            recv_sem=recv_sem.at[index],
            device_id=device,
            device_id_type=MESH,
        )
        copy.start()
        return copy

    for name in ("lat", "rope", "lgain", "tab"):
        loads[name].wait()
    base_cos = tab_ref[0, pl.ds(tokens + me, 1), :]
    base_sin = tab_ref[1, pl.ds(tokens + me, 1), :]
    cosine = tab_ref[0, :tokens, :] * base_cos - tab_ref[1, :tokens, :] * base_sin
    sine = tab_ref[1, :tokens, :] * base_cos + tab_ref[0, :tokens, :] * base_sin
    lat = lat_ref[...].astype(F32)
    mean = jnp.mean(lat * lat, axis=-1, keepdims=True)
    kv[0, :tokens, :] = (lat * lax.rsqrt(mean + EPS) * lgain_ref[...]).astype(BF16)
    wide = jnp.concatenate([rope_ref[...].astype(F32)] * (LANES // ROPE), axis=0)
    pad = -tokens % LANES
    if pad:
        wide = jnp.concatenate([wide, jnp.zeros((LANES, pad), F32)], axis=1)
    wide = jnp.transpose(wide)[:tokens]
    turned = wide * cosine + swapped(wide) * sine
    lane = lax.broadcasted_iota(jnp.int32, (packed, LANES), 1)
    masks = [(lane // ROPE == g).astype(F32) for g in range(LANES // ROPE)]
    strip = sum(turned[g * packed : (g + 1) * packed] * masks[g] for g in range(LANES // ROPE))
    rest = kv.shape[1] - tokens - packed
    if rest:
        strip = jnp.concatenate([strip, jnp.zeros((rest, LANES), F32)], axis=0)
    kv[0, tokens:, :] = strip.astype(BF16)

    pl.semaphore_wait(barrier, n + groups - 1)
    shared = {}
    for d in range(n - 1, 0, -1):
        shared[d] = remote(kv.at[0], kv.at[d], {"sp": partners(me, d, n)[0]})
    away = {}
    for j in range(1, groups):
        away[j] = remote(
            down_any, dw_ref.at[pl.ds(2 * j * hidden, hidden)], {"tp": lax.rem(rank + m - 2 * j, m)}
        )
    aside = [
        remote(gate_any, gu_ref.at[:, pl.ds(hidden, hidden)], {"tp": sibling}),
        remote(up_any, gu_ref.at[:, pl.ds(local + hidden, hidden)], {"tp": sibling}),
        remote(down_any, dw_ref.at[pl.ds(hidden, hidden)], {"tp": sibling}),
    ]

    factor = (NOPE + ROPE) ** (-0.5) * LOG2E
    loads["qr"].wait()
    rep_row = lax.broadcasted_iota(jnp.int32, (LANES, LANES * LANES // ROPE), 0)
    rep_col = lax.broadcasted_iota(jnp.int32, (LANES, LANES * LANES // ROPE), 1)
    spread = (
        rep_row == rep_col // LANES * ROPE + rep_col % ROPE
    ).astype(F32).astype(BF16)
    for g in range(HEADS * ROPE // LANES):
        x = qr_ref[:, g * LANES : (g + 1) * LANES].astype(F32)
        x = ((x * cosine + swapped(x) * sine) * factor).astype(BF16)
        x = jnp.dot(x, spread, preferred_element_type=F32).astype(BF16)
        for k in range(LANES // ROPE):
            head = g * (LANES // ROPE) + k
            query[head * tokens : (head + 1) * tokens, LATENT:] = x[:, k * LANES : (k + 1) * LANES]
    lane = lax.broadcasted_iota(jnp.int32, (tokens, LANES), 1)
    below = lane < NOPE
    lowb = below.astype(F32).astype(BF16)
    highb = (lane >= NOPE).astype(F32).astype(BF16)
    loads["qn"].wait()
    loads["upk"].wait()
    for g in range(HEADS * NOPE // LANES):
        plain = qn_ref[:, g * LANES : (g + 1) * LANES]
        pair = jnp.concatenate([plain * lowb, plain * highb], axis=0)
        absorbed = lax.dot_general(
            pair, upk_ref[:, g * LANES : (g + 1) * LANES], BYCOL, preferred_element_type=F32
        )
        query[2 * g * tokens : 2 * (g + 1) * tokens, :LATENT] = (absorbed * factor).astype(BF16)

    loads["picks"].wait()
    loads["share"].wait()
    spots = place(picks_ref, n, slots, tokens)
    packer[...] = sum(spots).astype(BF16)
    coarse = fine = 0.0
    for k in range(TOPK):
        share = share_ref[k : k + 1, :]
        rounded = share.astype(BF16).astype(F32)
        coarse = coarse + spots[k] * rounded
        fine = fine + spots[k] * (share - rounded)
    if pad:
        filler = jnp.zeros((n * slots, pad), F32)
        coarse = jnp.concatenate([coarse, filler], axis=1)
        fine = jnp.concatenate([fine, filler], axis=1)
    high[...] = jnp.transpose(coarse)[:tokens].astype(BF16)
    low[...] = jnp.transpose(fine)[:tokens].astype(BF16)

    vals[:, LATENT:] = jnp.ones((n * tokens, LANES), BF16)
    for d in [0] + list(range(1, n)):
        if d:
            shared[d].wait()
        rows = slice(d * tokens, (d + 1) * tokens)
        keys[rows, :LATENT] = kv[d, :tokens, :]
        vals[rows, :LATENT] = kv[d, :tokens, :]
        strip = kv[d, tokens:, :].astype(F32)[:packed]
        keys[rows, LATENT:] = jnp.concatenate([strip * mask for mask in masks], axis=0).astype(BF16)
    loads["upv"].wait()

    def heads(g, carry):
        lanes = pl.ds(pl.multiple_of(g * LANES, LANES), LANES)
        mine = query[pl.ds(pl.multiple_of(g * 2 * tokens, 2 * tokens), 2 * tokens), :]
        scores = lax.dot_general(mine, keys[...], BYCOL, preferred_element_type=F32)
        weights = jnp.exp2(scores - jnp.max(scores, axis=-1, keepdims=True)).astype(BF16)
        mixed = jnp.dot(weights, vals[...], preferred_element_type=F32)
        mixed = (mixed[:, :LATENT] / mixed[:, LATENT:]).astype(BF16)
        mixed = jnp.dot(mixed, upv_ref[:, lanes], preferred_element_type=F32)
        att[:, lanes] = jnp.where(below, mixed[:tokens], mixed[tokens:]).astype(BF16)
        return carry

    lax.fori_loop(0, HEADS * VDIM // LANES, heads, 0)
    loads["ow"].wait()
    loads["res"].wait()
    loads["fgain"].wait()

    def project(c, square):
        cols = pl.ds(pl.multiple_of(c * step, step), step)
        product = jnp.dot(att[...], ow_ref[:, cols], preferred_element_type=F32)
        middle = (mid_ref[:, cols].astype(F32) + product).astype(BF16)
        mid_ref[:, cols] = middle
        full = middle.astype(F32)
        return square + jnp.sum(full * full, axis=-1, keepdims=True)

    square = lax.fori_loop(0, width // step, project, jnp.zeros((tokens, 1), F32))
    scale = lax.rsqrt(square / width + EPS)
    norm[...] = (mid_ref[...].astype(F32) * scale * fgain_ref[...]).astype(BF16)

    def pack(c, carry):
        cols = pl.ds(pl.multiple_of(c * step, step), step)
        sent[:, cols] = jnp.dot(packer[...], norm[:, cols], preferred_element_type=F32).astype(BF16)
        return carry

    lax.fori_loop(0, width // step, pack, 0)

    def block(index):
        return pl.ds(pl.multiple_of(index * slots, slots), slots)

    arrive, across, crossed, returned = {}, {}, {}, {}
    for p, d in enumerate(order):
        if d:
            peer = partners(me, d, n)[0]
            arrive[d] = remote(sent.at[block(peer)], rows_a.at[block(p)], {"sp": peer})
    rows_a[(n - 1) * slots :, :] = sent[block(me), :]

    def forward(k):
        for p in range(k * count, (k + 1) * count):
            if order[p]:
                arrive[order[p]].wait()
            for j in range(1, groups):
                across[p, j] = remote(
                    rows_a.at[block(p)], rows_b.at[j - 1, block(p)], {"tp": lax.rem(rank + 2 * j, m)}
                )

    def gates(k):
        rows = pl.ds(k * span, span)
        for j in range(1, groups):
            for p in range(k * count, (k + 1) * count):
                across[p, j].wait()
        if k == 0:
            for name in ("gate", "up", "down"):
                loads[name].wait()
            for copy in aside:
                copy.wait()
            for j in range(1, groups):
                away[j].wait()
                away[-j] = remote(
                    dw_ref.at[pl.ds(2 * j * hidden, hidden)],
                    dw_ref.at[pl.ds((2 * j + 1) * hidden, hidden)],
                    {"tp": sibling},
                )
        stack = jnp.concatenate(
            [rows_a[rows, :]] + [rows_b[j - 1, rows, :] for j in range(1, groups)], axis=0
        )
        both = jnp.dot(stack, gu_ref[...], preferred_element_type=F32)
        gate = jnp.minimum(both[:, :local], CLAMP)
        lift = jnp.clip(both[:, local:], -CLAMP, CLAMP)
        active = (gate * jax.nn.sigmoid(ALPHA * gate) * (lift + 1.0)).astype(BF16)
        for j in range(1, groups):
            act_b[j - 1, rows, :] = active[j * span : (j + 1) * span]
            crossed[k, j] = remote(
                act_b.at[j - 1, rows],
                act.at[rows, pl.ds(j * local, local)],
                {"tp": lax.rem(rank + m - 2 * j, m)},
            )
        act[rows, :local] = active[:span]

    def lower(k):
        rows = pl.ds(k * span, span)
        for j in range(1, groups):
            crossed[k, j].wait()
            if k == 0:
                away[-j].wait()

        def down(c, carry):
            cols = pl.ds(pl.multiple_of(c * step, step), step)
            res[rows, cols] = jnp.dot(
                act[rows, :], dw_ref[:, cols], preferred_element_type=F32
            ).astype(BF16)
            return carry

        lax.fori_loop(0, width // step, down, 0)
        for p in range(k * count, (k + 1) * count):
            d = order[p]
            if d:
                returned[d] = remote(
                    res.at[block(p)], back.at[block(me)], {"sp": partners(me, d, n)[1]}
                )
            else:
                back[block(me), :] = res[p * slots : (p + 1) * slots, :]

    for t in range(parts + 2):
        for work, k in ((forward, t), (gates, t - 1), (lower, t - 2)):
            if 0 <= k < parts:
                work(k)
    for d in order:
        if d:
            returned[d].wait()

    def combine(c, carry):
        cols = pl.ds(pl.multiple_of(c * step, step), step)
        rows = back[:, cols]
        added = jnp.dot(high[...], rows, preferred_element_type=F32)
        added = added + jnp.dot(low[...], rows, preferred_element_type=F32)
        out_ref[:, cols] = (mid_ref[:, cols].astype(F32) + added).astype(BF16)
        return carry

    lax.fori_loop(0, width // step, combine, 0)


def rotary_tables(tokens, n):
    half = ROPE // 2
    lane = np.arange(LANES)
    inverse = ROPE_BASE ** (-(lane % half) * 2.0 / ROPE)
    places = np.concatenate([np.arange(tokens), np.arange(n) * tokens]).astype(np.float64)
    angle = places[:, None] * inverse[None, :]
    sign = np.where(lane % ROPE < half, -1.0, 1.0)[None, :]
    return np.stack([np.cos(angle), np.sin(angle) * sign]).astype(np.float32)


def local(
    residual, query_nope, query_rope, latent, rope_key, latent_gain, up_key, up_value,
    out_weight, ffn_gain, routes, route_weight, gate_weight, up_weight, down_weight,
):
    tokens, width = residual.shape[1:]
    hidden = gate_weight.shape[2]
    n = lax.axis_size("sp")
    m = lax.axis_size("tp")
    groups = m // 2
    parts = min(4, n)
    slots = min(tokens, max(2, 5 * tokens * TOPK // (4 * n)))
    slots = -(-slots // 16) * 16
    depth = tokens + tokens // (LANES // ROPE)
    depth = -(-depth // 16) * 16
    tables = jnp.asarray(rotary_tables(tokens, n))
    copies = 3 * (n - 1) + 3 + (groups - 1) * (2 + n + parts)

    def vmem(*shape, dtype=BF16):
        return pltpu.VMEM(shape, dtype)

    updated = pl.pallas_call(
        functools.partial(layer_kernel, n, m, slots, parts),
        out_shape=jax.ShapeDtypeStruct((tokens, width), BF16),
        in_specs=[ANY] * 16,
        out_specs=VM,
        scratch_shapes=[
            vmem(tokens, LATENT),
            vmem(ROPE, tokens),
            vmem(1, LATENT, dtype=F32),
            vmem(*tables.shape, dtype=F32),
            vmem(tokens, HEADS * NOPE),
            vmem(tokens, HEADS * ROPE),
            vmem(LATENT, HEADS * NOPE),
            vmem(LATENT, HEADS * VDIM),
            vmem(HEADS * VDIM, width),
            vmem(tokens, width),
            vmem(1, width, dtype=F32),
            vmem(TOPK, tokens, dtype=jnp.int32),
            vmem(TOPK, tokens, dtype=F32),
            vmem(width, 4 * hidden),
            vmem(m * hidden, width),
            vmem(n, depth, LANES),
            vmem(n * tokens, 2 * LANES),
            vmem(n * tokens, 2 * LANES),
            vmem(HEADS * tokens, 2 * LANES),
            vmem(tokens, HEADS * VDIM),
            vmem(tokens, width),
            vmem(n * slots, tokens),
            vmem(tokens, n * slots),
            vmem(tokens, n * slots),
            vmem(n * slots, width),
            vmem(n * slots, width),
            vmem(max(1, groups - 1), n * slots, width),
            vmem(n * slots, m * hidden),
            vmem(max(1, groups - 1), n * slots, 2 * hidden),
            vmem(n * slots, width),
            vmem(n * slots, width),
            pltpu.SemaphoreType.DMA((16,)),
            pltpu.SemaphoreType.DMA((copies,)),
            pltpu.SemaphoreType.DMA((copies,)),
        ],
        compiler_params=pltpu.CompilerParams(
            collective_id=0, has_side_effects=True, vmem_limit_bytes=60 * 2**20
        ),
    )(
        latent[0], jnp.transpose(rope_key[0]), latent_gain[None, :], tables, query_nope[0],
        query_rope[0], up_key, up_value, out_weight, residual[0], ffn_gain[None, :],
        jnp.transpose(routes, (0, 2, 1)), jnp.transpose(route_weight[0]),
        gate_weight[0], up_weight[0], down_weight[0],
    )
    return updated[None]


def solution(mesh):
    in_specs = (
        P("tp", "sp", None),
        P("tp", "sp", None),
        P("tp", "sp", None),
        P("tp", "sp", None),
        P("tp", "sp", None),
        P(),
        P(),
        P(),
        P(),
        P(),
        P(None, "sp", None),
        P("tp", "sp", None),
        P("sp", None, "tp"),
        P("sp", None, "tp"),
        P("sp", "tp", None),
    )
    out_specs = P("tp", "sp", None)
    return jax.shard_map(local, mesh=mesh, in_specs=in_specs, out_specs=out_specs, check_vma=False)
```

time: 113 us -> 80.7 us (0.71)
  Pallas kernels: 108 us -> 78.8 us
  local copies, waits for them, and re-layouts: 4.44 us -> 1.77 us
    pallas_call x3 -> x1, Pallas kernels: 108 us -> 78.8 us  [local(): pl.pallas_call(functools.partial(layer_kernel, n, m, slots, parts), out_s...]
    another operation x2 -> x0, local copies, waits for them, and re-layouts: 1.41 us -> none  [local(): jnp.tile(rope_key[0], (1, LANES // ROPE))]
    unnamed x3 -> x1, local copies, waits for them, and re-layouts: 2.45 us -> 1.77 us
where the time goes in v1:
time: 80.7 us; the launch traced here: 80.6 us
  Pallas kernels  78.8 us (98%)
  local copies, waits for them, and re-layouts  1.77 us (2%)
    pallas_call x1, Pallas kernels, local(): pl.pallas_call(functools.partial(layer_kernel, n, m, slots, parts), out_s...  78.8 us
    unnamed x1, local copies, waits for them, and re-layouts  1.77 us

profile of v1, /device:TPU:0, one launch (start us, length us, event | category | flops | bytes accessed | tf_op | source)
XLA Modules:
  0.0 80.6 jit_solution(9426659526007273862)
XLA Ops:
  0.0 78.8 %shard_map.154 = bf16[96,2048]{1,0:T(8,128)(2,1)} custom-call(bf16[96,128]{1,0:T(8,128)(2,1)} %bitcast.24, bf16[32,96]{1,0:T(8,128)(2,1)} %bitcast.25, f32[1,128]{1,0:T(1,128)} %bitcast.29, f32[2,104,128]{2,1,0:T(8,128)} %constant.2.clone.tab_any, bf16[96,1024]{1,0:T(8,128)(2,1)} %bitcast.22, bf16[96,512]{1,0:T(8,128)(2,1)} %bitcast.23, ...), custom_call_target="tpu_custom_call" | custom-call | tf_op jit(solution)/shard_map/pallas_call | solution.py:393
  78.8 1.8 %copy.18 = bf16[1,96,2048]{2,1,0:T(8,128)(2,1)} copy(bf16[1,96,2048]{2,1,0:T(8,128)(2,1)} %bitcast.17) | data formatting | bytes 786432

commit v2 on v1

--- a/solution.py
+++ b/solution.py
@@ -63,17 +63,25 @@
     return peer, peer
 
 
+def schedule(n):
+    quarter = n // 4
+    if n & (n - 1) or not quarter:
+        return list(range(n - 1, 0, -1)), list(range(n - 1, -1, -1))
+    own, near, mid, far = (list(range((q + 1) * quarter - 1, q * quarter - 1, -1)) for q in range(4))
+    return own[:-1] + far + near + mid, far + near + mid + own
+
+
 def layer_kernel(
     n, m, slots, parts,
     lat_any, rope_any, lgain_any, tab_any, qn_any, qr_any, upk_any, upv_any, ow_any, res_any,
     fgain_any, routes_any, share_any, gate_any, up_any, down_any,
-    out_ref,
+    mid_out, back, high_out, low_out,
     lat_ref, rope_ref, lgain_ref, tab_ref, qn_ref, qr_ref, upk_ref, upv_ref, ow_ref, mid_ref,
     fgain_ref, picks_ref, share_ref, gu_ref, dw_ref,
-    kv, keys, vals, query, att, norm, packer, high, low, sent, rows_a, rows_b, act, act_b, res, back,
-    load_sem, send_sem, recv_sem,
+    kv, keys, vals, query, partial, peaks, att, norm, packer, high, low, sent, rows_a, rows_b, act, act_b, res,
+    load_sem, save_sem, send_sem, recv_sem,
 ):
-    tokens, width = out_ref.shape
+    tokens, width = mid_out.shape
     hidden = gate_any.shape[1]
     groups = m // 2
     local = 2 * hidden
@@ -83,7 +91,7 @@
     count = n // parts
     span = count * slots
     step = 512
-    order = list(range(n - 1, -1, -1))
+    sending, order = schedule(n)
     packed = tokens // (LANES // ROPE)
 
     barrier = pltpu.get_barrier_semaphore()
@@ -120,6 +128,12 @@
     load("up", up_any, gu_ref.at[:, pl.ds(local, hidden)])
     load("down", down_any, dw_ref.at[pl.ds(0, hidden)])
 
+    saves = []
+
+    def save(source, target):
+        saves.append(pltpu.make_async_copy(source, target, save_sem.at[len(saves)]))
+        saves[-1].start()
+
     used = [0]
 
     def remote(source, target, device):
@@ -135,6 +149,13 @@
         )
         copy.start()
         return copy
+
+    pl.semaphore_wait(barrier, n + groups - 1)
+    away = {}
+    for j in range(1, groups):
+        away[j] = remote(
+            down_any, dw_ref.at[pl.ds(2 * j * hidden, hidden)], {"tp": lax.rem(rank + m - 2 * j, m)}
+        )
 
     for name in ("lat", "rope", "lgain", "tab"):
         loads[name].wait()
@@ -159,15 +180,9 @@
         strip = jnp.concatenate([strip, jnp.zeros((rest, LANES), F32)], axis=0)
     kv[0, tokens:, :] = strip.astype(BF16)
 
-    pl.semaphore_wait(barrier, n + groups - 1)
     shared = {}
-    for d in range(n - 1, 0, -1):
+    for d in range(1, n):
         shared[d] = remote(kv.at[0], kv.at[d], {"sp": partners(me, d, n)[0]})
-    away = {}
-    for j in range(1, groups):
-        away[j] = remote(
-            down_any, dw_ref.at[pl.ds(2 * j * hidden, hidden)], {"tp": lax.rem(rank + m - 2 * j, m)}
-        )
     aside = [
         remote(gate_any, gu_ref.at[:, pl.ds(hidden, hidden)], {"tp": sibling}),
         remote(up_any, gu_ref.at[:, pl.ds(local + hidden, hidden)], {"tp": sibling}),
@@ -218,9 +233,12 @@
         fine = jnp.concatenate([fine, filler], axis=1)
     high[...] = jnp.transpose(coarse)[:tokens].astype(BF16)
     low[...] = jnp.transpose(fine)[:tokens].astype(BF16)
+    save(high, high_out)
+    save(low, low_out)
 
     vals[:, LATENT:] = jnp.ones((n * tokens, LANES), BF16)
-    for d in [0] + list(range(1, n)):
+
+    def unpack(d):
         if d:
             shared[d].wait()
         rows = slice(d * tokens, (d + 1) * tokens)
@@ -228,20 +246,48 @@
         vals[rows, :LATENT] = kv[d, :tokens, :]
         strip = kv[d, tokens:, :].astype(F32)[:packed]
         keys[rows, LATENT:] = jnp.concatenate([strip * mask for mask in masks], axis=0).astype(BF16)
-    loads["upv"].wait()
-
-    def heads(g, carry):
+    early = max(1, n // 2) * tokens
+    total = n * tokens
+
+    def scored(g, start, size):
+        mine = query[pl.ds(pl.multiple_of(g * 2 * tokens, 2 * tokens), 2 * tokens), :]
+        return lax.dot_general(
+            mine, keys[start : start + size, :], BYCOL, preferred_element_type=F32
+        )
+
+    def first(g, carry):
+        rows = pl.ds(pl.multiple_of(g * 2 * tokens, 2 * tokens), 2 * tokens)
+        scores = scored(g, 0, early)
+        peak = jnp.max(scores, axis=-1, keepdims=True)
+        weights = jnp.exp2(scores - peak).astype(BF16)
+        partial[rows, :] = jnp.dot(weights, vals[:early, :], preferred_element_type=F32)
+        peaks[rows, :] = jnp.broadcast_to(peak, (2 * tokens, LANES))
+        return carry
+
+    def second(g, carry):
         lanes = pl.ds(pl.multiple_of(g * LANES, LANES), LANES)
-        mine = query[pl.ds(pl.multiple_of(g * 2 * tokens, 2 * tokens), 2 * tokens), :]
-        scores = lax.dot_general(mine, keys[...], BYCOL, preferred_element_type=F32)
-        weights = jnp.exp2(scores - jnp.max(scores, axis=-1, keepdims=True)).astype(BF16)
-        mixed = jnp.dot(weights, vals[...], preferred_element_type=F32)
-        mixed = (mixed[:, :LATENT] / mixed[:, LATENT:]).astype(BF16)
+        rows = pl.ds(pl.multiple_of(g * 2 * tokens, 2 * tokens), 2 * tokens)
+        scores = scored(g, early, total - early)
+        before = peaks[rows, :]
+        peak = jnp.maximum(before[:, :1], jnp.max(scores, axis=-1, keepdims=True))
+        weights = jnp.exp2(scores - peak).astype(BF16)
+        keep = jnp.exp2(before - peak)
+        mixed = jnp.dot(weights, vals[early:, :], preferred_element_type=F32)
+        above = mixed[:, :LATENT] + keep * partial[rows, :LATENT]
+        under = mixed[:, LATENT:] + keep * partial[rows, LATENT:]
+        mixed = (above / under).astype(BF16)
         mixed = jnp.dot(mixed, upv_ref[:, lanes], preferred_element_type=F32)
         att[:, lanes] = jnp.where(below, mixed[:tokens], mixed[tokens:]).astype(BF16)
         return carry
 
-    lax.fori_loop(0, HEADS * VDIM // LANES, heads, 0)
+    pairs = HEADS * VDIM // LANES
+    for d in range(early // tokens):
+        unpack(d)
+    lax.fori_loop(0, pairs, first, 0, unroll=4)
+    for d in range(early // tokens, n):
+        unpack(d)
+    loads["upv"].wait()
+    lax.fori_loop(0, pairs, second, 0, unroll=4)
     loads["ow"].wait()
     loads["res"].wait()
     loads["fgain"].wait()
@@ -254,26 +300,27 @@
         full = middle.astype(F32)
         return square + jnp.sum(full * full, axis=-1, keepdims=True)
 
-    square = lax.fori_loop(0, width // step, project, jnp.zeros((tokens, 1), F32))
+    square = lax.fori_loop(0, width // step, project, jnp.zeros((tokens, 1), F32), unroll=2)
     scale = lax.rsqrt(square / width + EPS)
     norm[...] = (mid_ref[...].astype(F32) * scale * fgain_ref[...]).astype(BF16)
+
+    save(mid_ref, mid_out)
 
     def pack(c, carry):
         cols = pl.ds(pl.multiple_of(c * step, step), step)
         sent[:, cols] = jnp.dot(packer[...], norm[:, cols], preferred_element_type=F32).astype(BF16)
         return carry
 
-    lax.fori_loop(0, width // step, pack, 0)
+    lax.fori_loop(0, width // step, pack, 0, unroll=2)
 
     def block(index):
         return pl.ds(pl.multiple_of(index * slots, slots), slots)
 
     arrive, across, crossed, returned = {}, {}, {}, {}
-    for p, d in enumerate(order):
-        if d:
-            peer = partners(me, d, n)[0]
-            arrive[d] = remote(sent.at[block(peer)], rows_a.at[block(p)], {"sp": peer})
-    rows_a[(n - 1) * slots :, :] = sent[block(me), :]
+    for d in sending:
+        peer = partners(me, d, n)[0]
+        arrive[d] = remote(sent.at[block(peer)], rows_a.at[block(order.index(d))], {"sp": peer})
+    rows_a[block(order.index(0)), :] = sent[block(me), :]
 
     def forward(k):
         for p in range(k * count, (k + 1) * count):
@@ -331,7 +378,7 @@
             ).astype(BF16)
             return carry
 
-        lax.fori_loop(0, width // step, down, 0)
+        lax.fori_loop(0, width // step, down, 0, unroll=True)
         for p in range(k * count, (k + 1) * count):
             d = order[p]
             if d:
@@ -339,7 +386,7 @@
                     res.at[block(p)], back.at[block(me)], {"sp": partners(me, d, n)[1]}
                 )
             else:
-                back[block(me), :] = res[p * slots : (p + 1) * slots, :]
+                save(res.at[block(p)], back.at[block(me)])
 
     for t in range(parts + 2):
         for work, k in ((forward, t), (gates, t - 1), (lower, t - 2)):
@@ -349,15 +396,47 @@
         if d:
             returned[d].wait()
 
-    def combine(c, carry):
-        cols = pl.ds(pl.multiple_of(c * step, step), step)
-        rows = back[:, cols]
-        added = jnp.dot(high[...], rows, preferred_element_type=F32)
-        added = added + jnp.dot(low[...], rows, preferred_element_type=F32)
+    for copy in saves:
+        copy.wait()
+
+
+def combine_kernel(
+    back_any, mid_any, high_any, low_any, out_any, back_ref, mid_ref, high_ref, low_ref, out_ref,
+    load_sem, save_sem,
+):
+    width = out_ref.shape[1]
+    chunks = save_sem.shape[0]
+    step = width // chunks
+    pieces = [pl.ds(c * step, step) for c in range(chunks)]
+    copies = [
+        pltpu.make_async_copy(high_any, high_ref, load_sem.at[0]),
+        pltpu.make_async_copy(low_any, low_ref, load_sem.at[1]),
+    ]
+    for c, cols in enumerate(pieces):
+        copies.append(
+            pltpu.make_async_copy(back_any.at[:, cols], back_ref.at[:, cols], load_sem.at[2 + 2 * c])
+        )
+        copies.append(
+            pltpu.make_async_copy(mid_any.at[:, cols], mid_ref.at[:, cols], load_sem.at[3 + 2 * c])
+        )
+    for copy in copies:
+        copy.start()
+    copies[0].wait()
+    copies[1].wait()
+    saves = []
+    for c, cols in enumerate(pieces):
+        copies[2 + 2 * c].wait()
+        copies[3 + 2 * c].wait()
+        rows = back_ref[:, cols]
+        added = jnp.dot(high_ref[...], rows, preferred_element_type=F32)
+        added = added + jnp.dot(low_ref[...], rows, preferred_element_type=F32)
         out_ref[:, cols] = (mid_ref[:, cols].astype(F32) + added).astype(BF16)
-        return carry
-
-    lax.fori_loop(0, width // step, combine, 0)
+        saves.append(
+            pltpu.make_async_copy(out_ref.at[:, cols], out_any.at[:, cols], save_sem.at[c])
+        )
+        saves[-1].start()
+    for copy in saves:
+        copy.wait()
 
 
 def rotary_tables(tokens, n):
@@ -379,7 +458,7 @@
     n = lax.axis_size("sp")
     m = lax.axis_size("tp")
     groups = m // 2
-    parts = min(4, n)
+    parts = min(8, n)
     slots = min(tokens, max(2, 5 * tokens * TOPK // (4 * n)))
     slots = -(-slots // 16) * 16
     depth = tokens + tokens // (LANES // ROPE)
@@ -390,11 +469,16 @@
     def vmem(*shape, dtype=BF16):
         return pltpu.VMEM(shape, dtype)
 
-    updated = pl.pallas_call(
+    middle, back, high, low = pl.pallas_call(
         functools.partial(layer_kernel, n, m, slots, parts),
-        out_shape=jax.ShapeDtypeStruct((tokens, width), BF16),
+        out_shape=(
+            jax.ShapeDtypeStruct((tokens, width), BF16),
+            jax.ShapeDtypeStruct((n * slots, width), BF16),
+            jax.ShapeDtypeStruct((tokens, n * slots), BF16),
+            jax.ShapeDtypeStruct((tokens, n * slots), BF16),
+        ),
         in_specs=[ANY] * 16,
-        out_specs=VM,
+        out_specs=(ANY,) * 4,
         scratch_shapes=[
             vmem(tokens, LATENT),
             vmem(ROPE, tokens),
@@ -415,6 +499,8 @@
             vmem(n * tokens, 2 * LANES),
             vmem(n * tokens, 2 * LANES),
             vmem(HEADS * tokens, 2 * LANES),
+            vmem(HEADS * tokens, 2 * LANES, dtype=F32),
+            vmem(HEADS * tokens, LANES, dtype=F32),
             vmem(tokens, HEADS * VDIM),
             vmem(tokens, width),
             vmem(n * slots, tokens),
@@ -426,8 +512,8 @@
             vmem(n * slots, m * hidden),
             vmem(max(1, groups - 1), n * slots, 2 * hidden),
             vmem(n * slots, width),
-            vmem(n * slots, width),
             pltpu.SemaphoreType.DMA((16,)),
+            pltpu.SemaphoreType.DMA((4,)),
             pltpu.SemaphoreType.DMA((copies,)),
             pltpu.SemaphoreType.DMA((copies,)),
         ],
@@ -440,6 +526,23 @@
         jnp.transpose(routes, (0, 2, 1)), jnp.transpose(route_weight[0]),
         gate_weight[0], up_weight[0], down_weight[0],
     )
+    chunks = max(1, width // 512)
+    updated = pl.pallas_call(
+        combine_kernel,
+        out_shape=jax.ShapeDtypeStruct((tokens, width), BF16),
+        in_specs=[ANY] * 4,
+        out_specs=ANY,
+        scratch_shapes=[
+            vmem(n * slots, width),
+            vmem(tokens, width),
+            vmem(tokens, n * slots),
+            vmem(tokens, n * slots),
+            vmem(tokens, width),
+            pltpu.SemaphoreType.DMA((2 + 2 * chunks,)),
+            pltpu.SemaphoreType.DMA((chunks,)),
+        ],
+        compiler_params=pltpu.CompilerParams(vmem_limit_bytes=60 * 2**20),
+    )(back, middle, high, low)
     return updated[None]
 
 

time: 80.7 us -> 70.9 us (0.88)
  Pallas kernels: 78.8 us -> 70.7 us
  local copies, waits for them, and re-layouts: 1.77 us -> 0 us
    pallas_call x1, Pallas kernels: 78.8 us -> 68 us  [local(): pl.pallas_call(functools.partial(layer_kernel, n, m, slots, parts), out_s...]
    pallas_call x0 -> x1, Pallas kernels: none -> 2.7 us  [local(): pl.pallas_call(combine_kernel, out_shape=jax.ShapeDtypeStruct((tokens, wi...]
    unnamed x1 -> x0, local copies, waits for them, and re-layouts: 1.77 us -> none
where the time goes in v2:
time: 70.9 us; the launch traced here: 70.7 us
  Pallas kernels  70.7 us (100%)
    pallas_call x1, Pallas kernels, local(): pl.pallas_call(functools.partial(layer_kernel, n, m, slots, parts), out_s...  68 us
    pallas_call x1, Pallas kernels, local(): pl.pallas_call(combine_kernel, out_shape=jax.ShapeDtypeStruct((tokens, wi...  2.7 us

profile of v2, /device:TPU:0, one launch (start us, length us, event | category | flops | bytes accessed | tf_op | source)
XLA Modules:
  0.0 70.7 jit_solution(15266267010243527849)
XLA Ops:
  0.0 68.0 %shard_map.154 = (bf16[96,2048]{1,0:T(8,128)(2,1)}, bf16[256,2048]{1,0:T(8,128)(2,1)}, bf16[96,256]{1,0:T(8,128)(2,1)}, bf16[96,256]{1,0:T(8,128)(2,1)}) custom-call(bf16[96,128]{1,0:T(8,128)(2,1)} %bitcast.23, bf16[32,96]{1,0:T(8,128)(2,1)} %bitcast.24, f32[1,128]{1,0:T(1,128)} %bitcast.28, f32[2,104,128]{2,1,0:T(8,128)} %constant.2.clone.tab_any, ...), custom_call_target="tpu_custom_call" | custom-call | tf_op jit(solution)/shard_map/pallas_call | solution.py:472
  68.0 2.7 %shard_map.155 = bf16[96,2048]{1,0:T(8,128)(2,1)} custom-call(bf16[256,2048]{1,0:T(8,128)(2,1)} %get-tuple-element.9.back_any, bf16[96,2048]{1,0:T(8,128)(2,1)} %get-tuple-element.10.mid_any, bf16[96,256]{1,0:T(8,128)(2,1)} %get-tuple-element.11.high_any, bf16[96,256]{1,0:T(8,128)(2,1)} %get-tuple-element.12.low_any), custom_call_target="tpu_custom_call" | custom-call | tf_op jit(solution)/shard_map/pallas_call | solution.py:530

commit v3 on v2

v3 whole, which is shorter than its diff:
```python
import functools

import jax
import jax.numpy as jnp
import numpy as np
from jax import lax
from jax.experimental import pallas as pl
from jax.experimental.pallas import tpu as pltpu
from jax.sharding import PartitionSpec as P

HEADS = 16
NOPE = 64
ROPE = 32
VDIM = 64
LATENT = 128
TOPK = 2
LANES = 128

EPS = 1e-06
ROPE_BASE = 10000.0
CLAMP = 7.0
ALPHA = 1.702
LOG2E = 1.4426950408889634
MESH = pl.DeviceIdType.MESH
VM = pl.BlockSpec(memory_space=pltpu.VMEM)
ANY = pl.BlockSpec(memory_space=pl.ANY)
HBM = pl.BlockSpec(memory_space=pltpu.HBM)
F32 = jnp.float32
BF16 = jnp.bfloat16
BYCOL = (((1,), (1,)), ((), ()))


def swapped(x):
    lane = lax.broadcasted_iota(jnp.int32, x.shape, 1)
    half = ROPE // 2
    return jnp.where(
        lane % ROPE < half, pltpu.roll(x, x.shape[1] - half, 1), pltpu.roll(x, half, 1)
    )


def place(picks_ref, experts, slots, tokens):
    expert = lax.broadcasted_iota(jnp.int32, (experts, tokens), 0)
    hots = [(expert == picks_ref[k : k + 1, :]).astype(F32) for k in range(TOPK)]
    earlier = (
        lax.broadcasted_iota(jnp.int32, (tokens, tokens), 0)
        < lax.broadcasted_iota(jnp.int32, (tokens, tokens), 1)
    ).astype(F32)
    rank = jnp.dot(sum(hots), earlier, preferred_element_type=F32)
    where = rank + (expert * slots).astype(F32)
    slot = lax.broadcasted_iota(jnp.int32, (experts * slots, tokens), 0).astype(F32)
    return [
        (slot == jnp.sum(hot * where, axis=0, keepdims=True)).astype(F32) for hot in hots
    ]


def partners(me, d, n):
    if n & (n - 1):
        return lax.rem(me + d, n), lax.rem(me + n - d, n)
    peer, bit = me, 1
    while bit < n:
        if d & bit:
            peer = peer + bit * (1 - 2 * lax.rem(lax.div(me, bit), 2))
        bit *= 2
    return peer, peer


def schedule(n):
    quarter = n // 4
    if n & (n - 1) or not quarter:
        return list(range(n - 1, 0, -1)), list(range(n - 1, -1, -1))
    own, near, mid, far = (list(range((q + 1) * quarter - 1, q * quarter - 1, -1)) for q in range(4))
    mixed = near[:1] + [d for pair in zip(mid, near[1:]) for d in pair] + mid[len(near) - 1 :]
    return own[:-1] + far + near + mid, far + mixed + own


def layer_kernel(
    n, m, slots, parts,
    lat_any, rope_any, lgain_any, tab_any, qn_any, qr_any, upk_any, upv_any, ow_any, res_any,
    fgain_any, routes_any, share_any, gate_any, up_any, down_any,
    mid_ref, back, high, low,
    lat_ref, rope_ref, lgain_ref, tab_ref, qn_ref, qr_ref, upk_ref, upv_ref, ow_ref,
    fgain_ref, picks_ref, share_ref, gu_ref, dw_ref,
    kv, keys, vals, query, partial, peaks, att, norm, packer, sent, rows_a, rows_b, act, act_b, res,
    load_sem, send_sem, recv_sem,
):
    tokens, width = mid_ref.shape
    hidden = gate_any.shape[1]
    groups = m // 2
    local = 2 * hidden
    me = lax.axis_index("sp")
    rank = lax.axis_index("tp")
    sibling = rank + 1 - 2 * lax.rem(rank, 2)
    count = n // parts
    span = count * slots
    step = 512
    sending, order = schedule(n)
    packed = tokens // (LANES // ROPE)

    barrier = pltpu.get_barrier_semaphore()
    for d in range(1, n):
        pl.semaphore_signal(
            barrier, inc=1, device_id={"sp": partners(me, d, n)[0]}, device_id_type=MESH
        )
    for j in range(1, groups):
        pl.semaphore_signal(
            barrier, inc=1, device_id={"tp": lax.rem(rank + 2 * j, m)}, device_id_type=MESH
        )
    pl.semaphore_signal(barrier, inc=1, device_id={"tp": sibling}, device_id_type=MESH)

    loads = [[] for _ in range(5)]

    def load(group, source, target):
        index = sum(len(copies) for copies in loads)
        copy = pltpu.make_async_copy(source, target, load_sem.at[index])
        copy.start()
        loads[group].append(copy)

    def loaded(group):
        for copy in loads[group]:
            copy.wait()

    load(0, lat_any, lat_ref)
    load(0, rope_any, rope_ref)
    load(0, lgain_any, lgain_ref)
    load(0, tab_any, tab_ref)
    load(1, qr_any, qr_ref)
    load(1, qn_any, qn_ref)
    load(1, upk_any, upk_ref)
    load(1, routes_any.at[rank], picks_ref)
    load(1, share_any, share_ref)
    load(2, upv_any, upv_ref)
    load(3, ow_any, ow_ref)
    load(3, res_any, mid_ref)
    load(3, fgain_any, fgain_ref)
    load(4, gate_any, gu_ref.at[:, pl.ds(0, hidden)])
    load(4, up_any, gu_ref.at[:, pl.ds(local, hidden)])
    load(4, down_any, dw_ref.at[pl.ds(0, hidden)])

    used = [0]

    def fresh(count=1):
        used[0] += count
        return used[0] - count

    def remote(source, target, device, leaves, index=None):
        copy = pltpu.make_async_remote_copy(
            src_ref=source,
            dst_ref=target,
            send_sem=send_sem.at[leaves],
            recv_sem=recv_sem.at[fresh() if index is None else index],
            device_id=device,
            device_id_type=MESH,
        )
        copy.start()
        return copy

    def together(extent, index, semaphores):
        pltpu.make_async_copy(extent, extent, semaphores.at[index]).wait()

    kv_out, aside_out, rows_out, back_out = range(4)
    away_out, relay_out, across_out, act_out = (4 + q * (groups - 1) - 1 for q in range(4))

    pl.semaphore_wait(barrier, n + groups - 1)
    away = {}
    for j in range(1, groups):
        away[j] = remote(
            down_any, dw_ref.at[pl.ds(2 * j * hidden, hidden)], {"tp": lax.rem(rank + m - 2 * j, m)},
            away_out + j,
        )

    loaded(0)
    base_cos = tab_ref[0, pl.ds(tokens + me, 1), :]
    base_sin = tab_ref[1, pl.ds(tokens + me, 1), :]
    cosine = tab_ref[0, :tokens, :] * base_cos - tab_ref[1, :tokens, :] * base_sin
    sine = tab_ref[1, :tokens, :] * base_cos + tab_ref[0, :tokens, :] * base_sin
    lat = lat_ref[...].astype(F32)
    mean = jnp.mean(lat * lat, axis=-1, keepdims=True)
    kv[0, :tokens, :] = (lat * lax.rsqrt(mean + EPS) * lgain_ref[...]).astype(BF16)
    wide = jnp.concatenate([rope_ref[...].astype(F32)] * (LANES // ROPE), axis=0)
    pad = -tokens % LANES
    if pad:
        wide = jnp.concatenate([wide, jnp.zeros((LANES, pad), F32)], axis=1)
    wide = jnp.transpose(wide)[:tokens]
    turned = wide * cosine + swapped(wide) * sine
    lane = lax.broadcasted_iota(jnp.int32, (packed, LANES), 1)
    masks = [(lane // ROPE == g).astype(F32) for g in range(LANES // ROPE)]
    strip = sum(turned[g * packed : (g + 1) * packed] * masks[g] for g in range(LANES // ROPE))
    rest = kv.shape[1] - tokens - packed
    if rest:
        strip = jnp.concatenate([strip, jnp.zeros((rest, LANES), F32)], axis=0)
    kv[0, tokens:, :] = strip.astype(BF16)

    shared, soon, late = {}, fresh(), fresh()
    for d in range(1, n):
        half = soon if d < max(1, n // 2) else late
        shared[d] = remote(kv.at[0], kv.at[d], {"sp": partners(me, d, n)[0]}, kv_out, half)
    pack_sem, back_sem = fresh(), fresh()
    aside = [
        remote(gate_any, gu_ref.at[:, pl.ds(hidden, hidden)], {"tp": sibling}, aside_out, pack_sem),
        remote(up_any, gu_ref.at[:, pl.ds(local + hidden, hidden)], {"tp": sibling}, aside_out, pack_sem),
        remote(down_any, dw_ref.at[pl.ds(hidden, hidden)], {"tp": sibling}, aside_out, pack_sem),
    ]

    factor = (NOPE + ROPE) ** (-0.5) * LOG2E
    loaded(1)
    rep_row = lax.broadcasted_iota(jnp.int32, (LANES, LANES * LANES // ROPE), 0)
    rep_col = lax.broadcasted_iota(jnp.int32, (LANES, LANES * LANES // ROPE), 1)
    spread = (
        rep_row == rep_col // LANES * ROPE + rep_col % ROPE
    ).astype(F32).astype(BF16)
    for g in range(HEADS * ROPE // LANES):
        x = qr_ref[:, g * LANES : (g + 1) * LANES].astype(F32)
        x = ((x * cosine + swapped(x) * sine) * factor).astype(BF16)
        x = jnp.dot(x, spread, preferred_element_type=F32).astype(BF16)
        for k in range(LANES // ROPE):
            head = g * (LANES // ROPE) + k
            query[head * tokens : (head + 1) * tokens, LATENT:] = x[:, k * LANES : (k + 1) * LANES]
    lane = lax.broadcasted_iota(jnp.int32, (tokens, LANES), 1)
    below = lane < NOPE
    lowb = below.astype(F32).astype(BF16)
    highb = (lane >= NOPE).astype(F32).astype(BF16)
    for g in range(HEADS * NOPE // LANES):
        plain = qn_ref[:, g * LANES : (g + 1) * LANES]
        pair = jnp.concatenate([plain * lowb, plain * highb], axis=0)
        absorbed = lax.dot_general(
            pair, upk_ref[:, g * LANES : (g + 1) * LANES], BYCOL, preferred_element_type=F32
        )
        query[2 * g * tokens : 2 * (g + 1) * tokens, :LATENT] = (absorbed * factor).astype(BF16)

    spots = place(picks_ref, n, slots, tokens)
    packer[...] = sum(spots).astype(BF16)
    coarse = fine = 0.0
    for k in range(TOPK):
        share = share_ref[k : k + 1, :]
        rounded = share.astype(BF16).astype(F32)
        coarse = coarse + spots[k] * rounded
        fine = fine + spots[k] * (share - rounded)
    if pad:
        filler = jnp.zeros((n * slots, pad), F32)
        coarse = jnp.concatenate([coarse, filler], axis=1)
        fine = jnp.concatenate([fine, filler], axis=1)
    high[...] = jnp.transpose(coarse)[:tokens].astype(BF16)
    low[...] = jnp.transpose(fine)[:tokens].astype(BF16)

    vals[:, LATENT:] = jnp.ones((n * tokens, LANES), BF16)

    def unpack(d):
        rows = slice(d * tokens, (d + 1) * tokens)
        keys[rows, :LATENT] = kv[d, :tokens, :]
        vals[rows, :LATENT] = kv[d, :tokens, :]
        strip = kv[d, tokens:, :].astype(F32)[:packed]
        keys[rows, LATENT:] = jnp.concatenate([strip * mask for mask in masks], axis=0).astype(BF16)
    soonest = max(1, n // 2)
    early = soonest * tokens
    total = n * tokens

    quad = 4 * tokens

    def scored(g, start, size):
        mine = query[pl.ds(pl.multiple_of(g * quad, quad), quad), :]
        return lax.dot_general(
            mine, keys[start : start + size, :], BYCOL, preferred_element_type=F32
        )

    def first(g, carry):
        rows = pl.ds(pl.multiple_of(g * quad, quad), quad)
        scores = scored(g, 0, early)
        peak = jnp.max(scores, axis=-1, keepdims=True)
        weights = jnp.exp2(scores - peak).astype(BF16)
        partial[rows, :] = jnp.dot(weights, vals[:early, :], preferred_element_type=F32)
        peaks[rows, :] = jnp.broadcast_to(peak, (quad, LANES))
        return carry

    def second(g, carry):
        rows = pl.ds(pl.multiple_of(g * quad, quad), quad)
        scores = scored(g, early, total - early)
        before = peaks[rows, :]
        peak = jnp.max(scores, axis=-1, keepdims=True)
        peak = jnp.maximum(before, jnp.broadcast_to(peak, before.shape))
        level = jnp.concatenate([peak] * -(-scores.shape[1] // LANES), axis=1)
        weights = jnp.exp2(scores - level[:, : scores.shape[1]]).astype(BF16)
        keep = jnp.exp2(before - peak)
        mixed = jnp.dot(weights, vals[early:, :], preferred_element_type=F32)
        above = mixed[:, :LATENT] + keep * partial[rows, :LATENT]
        under = mixed[:, LATENT:] + keep * partial[rows, LATENT:]
        mixed = above.astype(BF16)
        for q in range(2):
            lanes = pl.ds(pl.multiple_of((g * 2 + q) * LANES, LANES), LANES)
            part = mixed[2 * q * tokens : 2 * (q + 1) * tokens]
            part = jnp.dot(part, upv_ref[:, lanes], preferred_element_type=F32)
            over = under[2 * q * tokens : 2 * (q + 1) * tokens]
            part = jnp.where(below, part[:tokens], part[tokens:])
            over = jnp.where(below, over[:tokens], over[tokens:])
            att[:, lanes] = (part / over).astype(BF16)
        return carry

    pairs = HEADS // 4
    if soonest > 1:
        together(kv.at[pl.ds(1, soonest - 1)], soon, recv_sem)
    for d in range(soonest):
        unpack(d)
    lax.fori_loop(0, pairs, first, 0, unroll=True)
    together(kv.at[pl.ds(soonest, n - soonest)], late, recv_sem)
    for d in range(soonest, n):
        unpack(d)
    loaded(2)
    lax.fori_loop(0, pairs, second, 0, unroll=2)
    loaded(3)

    def project(c, square):
        cols = pl.ds(pl.multiple_of(c * step, step), step)
        product = jnp.dot(att[...], ow_ref[:, cols], preferred_element_type=F32)
        middle = (mid_ref[:, cols].astype(F32) + product).astype(BF16)
        mid_ref[:, cols] = middle
        full = middle.astype(F32)
        return square + jnp.sum(full * full, axis=-1, keepdims=True)

    square = lax.fori_loop(0, width // step, project, jnp.zeros((tokens, 1), F32), unroll=2)
    scale = lax.rsqrt(square / width + EPS)
    norm[...] = (mid_ref[...].astype(F32) * scale * fgain_ref[...]).astype(BF16)


    def pack(c, carry):
        cols = pl.ds(pl.multiple_of(c * step, step), step)
        sent[:, cols] = jnp.dot(packer[...], norm[:, cols], preferred_element_type=F32).astype(BF16)
        return carry

    lax.fori_loop(0, width // step, pack, 0, unroll=2)

    def block(index):
        return pl.ds(pl.multiple_of(index * slots, slots), slots)

    arrive, across, crossed, returned = {}, {}, {}, {}
    for d in sending:
        peer = partners(me, d, n)[0]
        arrive[d] = remote(sent.at[block(peer)], rows_a.at[block(order.index(d))], {"sp": peer}, rows_out)
    rows_a[block(order.index(0)), :] = sent[block(me), :]

    def forward(k):
        for p in range(k * count, (k + 1) * count):
            if order[p]:
                arrive[order[p]].wait_recv()
            for j in range(1, groups):
                across[p, j] = remote(
                    rows_a.at[block(p)], rows_b.at[j - 1, block(p)], {"tp": lax.rem(rank + 2 * j, m)},
                    across_out + j,
                )

    def gates(k):
        rows = pl.ds(k * span, span)
        for j in range(1, groups):
            for p in range(k * count, (k + 1) * count):
                across[p, j].wait_recv()
        if k == 0:
            loaded(4)
            together(dw_ref.at[pl.ds(0, 3 * hidden)], pack_sem, recv_sem)
            for j in range(1, groups):
                away[j].wait_recv()
                away[-j] = remote(
                    dw_ref.at[pl.ds(2 * j * hidden, hidden)],
                    dw_ref.at[pl.ds((2 * j + 1) * hidden, hidden)],
                    {"tp": sibling},
                    relay_out + j,
                )
        stack = jnp.concatenate(
            [rows_a[rows, :]] + [rows_b[j - 1, rows, :] for j in range(1, groups)], axis=0
        )
        both = jnp.dot(stack, gu_ref[...], preferred_element_type=F32)
        gate = jnp.minimum(both[:, :local], CLAMP)
        lift = jnp.clip(both[:, local:], -CLAMP, CLAMP)
        active = (gate * jax.nn.sigmoid(ALPHA * gate) * (lift + 1.0)).astype(BF16)
        for j in range(1, groups):
            act_b[j - 1, rows, :] = active[j * span : (j + 1) * span]
            crossed[k, j] = remote(
                act_b.at[j - 1, rows],
                act.at[rows, pl.ds(j * local, local)],
                {"tp": lax.rem(rank + m - 2 * j, m)},
                act_out + j,
            )
        act[rows, :local] = active[:span]

    def lower(k):
        rows = pl.ds(k * span, span)
        for j in range(1, groups):
            crossed[k, j].wait_recv()
            if k == 0:
                away[-j].wait_recv()

        def down(c, carry):
            cols = pl.ds(pl.multiple_of(c * step, step), step)
            res[rows, cols] = jnp.dot(
                act[rows, :], dw_ref[:, cols], preferred_element_type=F32
            ).astype(BF16)
            return carry

        lax.fori_loop(0, width // step, down, 0, unroll=True)
        for p in range(k * count, (k + 1) * count):
            d = order[p]
            if d:
                returned[d] = remote(
                    res.at[block(p)], back.at[block(me)], {"sp": partners(me, d, n)[1]}, back_out,
                    back_sem,
                )
            else:
                back[block(me), :] = res[p * slots : (p + 1) * slots, :]

    for t in range(parts + 2):
        for work, k in ((forward, t), (gates, t - 1), (lower, t - 2)):
            if 0 <= k < parts:
                work(k)
    others = pl.ds(0, (n - 1) * slots)
    together(back.at[others], back_sem, recv_sem)
    together(kv.at[pl.ds(0, n - 1)], kv_out, send_sem)
    together(dw_ref.at[pl.ds(0, 3 * hidden)], aside_out, send_sem)
    together(rows_a.at[others], rows_out, send_sem)
    together(back.at[others], back_out, send_sem)
    for j in range(1, groups):
        together(dw_ref.at[pl.ds(0, hidden)], away_out + j, send_sem)
        together(dw_ref.at[pl.ds(0, hidden)], relay_out + j, send_sem)
        together(rows_a, across_out + j, send_sem)
        together(act_b.at[j - 1], act_out + j, send_sem)


def combine_kernel(back_ref, mid_ref, high_ref, low_ref, out_any, out_ref, save_sem):
    width = out_ref.shape[1]
    chunks = save_sem.shape[0]
    step = width // chunks
    saves = []
    for c in range(chunks):
        cols = pl.ds(c * step, step)
        rows = back_ref[:, cols]
        added = jnp.dot(high_ref[...], rows, preferred_element_type=F32)
        added = added + jnp.dot(low_ref[...], rows, preferred_element_type=F32)
        out_ref[:, cols] = (mid_ref[:, cols].astype(F32) + added).astype(BF16)
        saves.append(
            pltpu.make_async_copy(out_ref.at[:, cols], out_any.at[:, cols], save_sem.at[c])
        )
        saves[-1].start()
    for copy in saves:
        copy.wait()


def rotary_tables(tokens, n):
    half = ROPE // 2
    lane = np.arange(LANES)
    inverse = ROPE_BASE ** (-(lane % half) * 2.0 / ROPE)
    places = np.concatenate([np.arange(tokens), np.arange(n) * tokens]).astype(np.float64)
    angle = places[:, None] * inverse[None, :]
    sign = np.where(lane % ROPE < half, -1.0, 1.0)[None, :]
    return np.stack([np.cos(angle), np.sin(angle) * sign]).astype(np.float32)


def local(
    residual, query_nope, query_rope, latent, rope_key, latent_gain, up_key, up_value,
    out_weight, ffn_gain, routes, route_weight, gate_weight, up_weight, down_weight,
):
    tokens, width = residual.shape[1:]
    hidden = gate_weight.shape[2]
    n = lax.axis_size("sp")
    m = lax.axis_size("tp")
    groups = m // 2
    parts = min(8, n)
    slots = min(tokens, max(2, 5 * tokens * TOPK // (4 * n)))
    slots = -(-slots // 16) * 16
    depth = tokens + tokens // (LANES // ROPE)
    depth = -(-depth // 16) * 16
    tables = jnp.asarray(rotary_tables(tokens, n))
    signals = n - 1 + 4 + (groups - 1) * (2 + n + parts)
    leaving = 4 * groups

    room = [16 * 2**20]

    def vmem(*shape, dtype=BF16):
        room[0] += int(np.prod(shape)) * jnp.dtype(dtype).itemsize
        return pltpu.VMEM(shape, dtype)

    scratch = [
        vmem(tokens, LATENT),
        vmem(ROPE, tokens),
        vmem(1, LATENT, dtype=F32),
        vmem(*tables.shape, dtype=F32),
        vmem(tokens, HEADS * NOPE),
        vmem(tokens, HEADS * ROPE),
        vmem(LATENT, HEADS * NOPE),
        vmem(LATENT, HEADS * VDIM),
        vmem(HEADS * VDIM, width),
        vmem(1, width, dtype=F32),
        vmem(TOPK, tokens, dtype=jnp.int32),
        vmem(TOPK, tokens, dtype=F32),
        vmem(width, 4 * hidden),
        vmem(m * hidden, width),
        vmem(n, depth, LANES),
        vmem(n * tokens, 2 * LANES),
        vmem(n * tokens, 2 * LANES),
        vmem(HEADS * tokens, 2 * LANES),
        vmem(HEADS * tokens, 2 * LANES, dtype=F32),
        vmem(HEADS * tokens, LANES, dtype=F32),
        vmem(tokens, HEADS * VDIM),
        vmem(tokens, width),
        vmem(n * slots, tokens),
        vmem(n * slots, width),
        vmem(n * slots, width),
        vmem(max(1, groups - 1), n * slots, width),
        vmem(n * slots, m * hidden),
        vmem(max(1, groups - 1), n * slots, 2 * hidden),
        vmem(n * slots, width),
        pltpu.SemaphoreType.DMA((16,)),
        pltpu.SemaphoreType.DMA((leaving,)),
        pltpu.SemaphoreType.DMA((signals,)),
    ]
    room = min(room[0], 60 * 2**20)
    arrays = (
        latent[0], jnp.transpose(rope_key[0]), latent_gain[None, :], tables, query_nope[0],
        query_rope[0], up_key, up_value, out_weight, residual[0], ffn_gain[None, :],
        jnp.transpose(routes, (0, 2, 1)), jnp.transpose(route_weight[0]),
        gate_weight[0], up_weight[0], down_weight[0],
    )
    middle, back, high, low = pl.pallas_call(
        functools.partial(layer_kernel, n, m, slots, parts),
        out_shape=(
            jax.ShapeDtypeStruct((tokens, width), BF16),
            jax.ShapeDtypeStruct((n * slots, width), BF16),
            jax.ShapeDtypeStruct((tokens, n * slots), BF16),
            jax.ShapeDtypeStruct((tokens, n * slots), BF16),
        ),
        in_specs=[HBM] * 16,
        out_specs=(VM,) * 4,
        scratch_shapes=scratch,
        compiler_params=pltpu.CompilerParams(
            collective_id=0, has_side_effects=True, vmem_limit_bytes=room
        ),
    )(*(pltpu.with_memory_space_constraint(x, pltpu.HBM) for x in arrays))
    chunks = max(1, width // 512)
    updated = pl.pallas_call(
        combine_kernel,
        out_shape=jax.ShapeDtypeStruct((tokens, width), BF16),
        in_specs=[VM] * 4,
        out_specs=HBM,
        scratch_shapes=[pltpu.VMEM((tokens, width), BF16), pltpu.SemaphoreType.DMA((chunks,))],
        compiler_params=pltpu.CompilerParams(vmem_limit_bytes=16 * 2**20),
    )(back, middle, high, low)
    return updated[None]


def solution(mesh):
    in_specs = (
        P("tp", "sp", None),
        P("tp", "sp", None),
        P("tp", "sp", None),
        P("tp", "sp", None),
        P("tp", "sp", None),
        P(),
        P(),
        P(),
        P(),
        P(),
        P(None, "sp", None),
        P("tp", "sp", None),
        P("sp", None, "tp"),
        P("sp", None, "tp"),
        P("sp", "tp", None),
    )
    out_specs = P("tp", "sp", None)
    return jax.shard_map(local, mesh=mesh, in_specs=in_specs, out_specs=out_specs, check_vma=False)
```

time: 70.9 us -> 65.2 us (0.920)
  Pallas kernels: 70.7 us -> 65.1 us
    pallas_call x1, Pallas kernels: 68 us -> 63.9 us  [local(): pl.pallas_call(functools.partial(layer_kernel, n, m, slots, parts), out_s...]
    pallas_call x1, Pallas kernels: 2.7 us -> 1.15 us  [local(): pl.pallas_call(combine_kernel, out_shape=jax.ShapeDtypeStruct((tokens, wi...]
where the time goes in v3:
time: 65.2 us; the launch traced here: 65.1 us
  Pallas kernels  65.1 us (100%)
    pallas_call x1, Pallas kernels, local(): pl.pallas_call(functools.partial(layer_kernel, n, m, slots, parts), out_s...  63.9 us

profile of v3, /device:TPU:0, one launch (start us, length us, event | category | flops | bytes accessed | tf_op | source)
XLA Modules:
  0.0 65.1 jit_solution(6646754314246464146)
XLA Ops:
  0.0 63.9 %shard_map.154 = (bf16[96,2048]{1,0:T(8,128)(2,1)S(1)}, bf16[256,2048]{1,0:T(8,128)(2,1)S(1)}, bf16[96,256]{1,0:T(8,128)(2,1)S(1)}, bf16[96,256]{1,0:T(8,128)(2,1)S(1)}) custom-call(bf16[96,128]{1,0:T(8,128)(2,1)} %bitcast.23, bf16[32,96]{1,0:T(8,128)(2,1)} %bitcast.24, f32[1,128]{1,0:T(1,128)} %bitcast.28, f32[2,104,128]{2,1,0:T(8,128)} %constant.2.clone.tab_any, ...), custom_call_target="tpu_custom_call" | custom-call | tf_op jit(solution)/shard_map/pallas_call | solution.py:518
  64.0 1.1 %shard_map.155 = bf16[96,2048]{1,0:T(8,128)(2,1)} custom-call(bf16[256,2048]{1,0:T(8,128)(2,1)S(1)} %get-tuple-element.9.back_ref, bf16[96,2048]{1,0:T(8,128)(2,1)S(1)} %get-tuple-element.10.mid_ref, bf16[96,256]{1,0:T(8,128)(2,1)S(1)} %get-tuple-element.11.high_ref, bf16[96,256]{1,0:T(8,128)(2,1)S(1)} %get-tuple-element.12.low_ref), custom_call_target="tpu_custom_call" | custom-call | tf_op jit(solution)/shard_map/pallas_call | solution.py:534
